TPU v7x, 32 devices: a whole 2x2x4 slice. The times are simulated.
32 devices in a mesh: sp: 16 (over z, y, x), tp: 2 (over core).
Axes of the slice: x: 2, y: 2, z: 4, core: 2. Of those that a mesh axis runs over, the one named last changes fastest.
Arguments:
- mixer_output: bfloat16 [2048, 2048], P('sp'), may hold values from -6 to 6
- layer_cotangent: bfloat16 [2048, 2048], P('sp'), may hold values from -6 to 6
- expert_choice: int32 [2048, 2], P('sp'), may hold values from 0 to 15, all different within a row; in each aligned block of 128 rows (0 to 127, 128 to 255, ...) at most 32 rows name the same one
- route_weight: float32 [2048, 2], P('sp'), may hold values from 0.1 to 0.9
- gate_pre: bfloat16 [16, 512, 1024], P('sp', None, 'tp'), may hold values from -15 to 15
- up_pre: bfloat16 [16, 512, 1024], P('sp', None, 'tp'), may hold values from -15 to 15
- w_gate: bfloat16 [16, 2048, 1024], P('sp', None, 'tp'), may hold values from -0.125 to 0.125
- w_up: bfloat16 [16, 2048, 1024], P('sp', None, 'tp'), may hold values from -0.125 to 0.125
- w_down: bfloat16 [16, 1024, 2048], P('sp', 'tp'), may hold values from -0.1875 to 0.1875
- w_out: bfloat16 [2048, 2048], P('tp'), may hold values from -0.125 to 0.125
- norm_gain: bfloat16 [2048], P('tp'), may hold values from 0.099609375 to 1.8984375
- scan_in: bfloat16 [2048, 2048], P('sp', 'tp'), may hold values from -6 to 6
- gate_in: bfloat16 [2048, 2048], P('sp', 'tp'), may hold values from -9 to 9
- b_proj: bfloat16 [2048, 1024], P('sp', 'tp'), may hold values from -1.796875 to 1.796875
- c_proj: bfloat16 [2048, 1024], P('sp', 'tp'), may hold values from -1.796875 to 1.796875
- log_decay: float32 [2048, 32], P('sp', 'tp'), may hold values from -3 to 0
- entry_state: float32 [16, 32, 64, 128], P('sp', 'tp'), may hold values from -24 to 24
Outputs:
- grad_w_gate: bfloat16 [16, 2048, 1024], P('sp', None, 'tp')
- grad_w_up: bfloat16 [16, 2048, 1024], P('sp', None, 'tp')
- grad_w_down: bfloat16 [16, 1024, 2048], P('sp', 'tp')
- grad_out_proj: float32 [2048, 2048], P('sp', 'tp')
- grad_scan_in: bfloat16 [2048, 2048], P('sp', 'tp')
- grad_gate_in: bfloat16 [2048, 2048], P('sp', 'tp')
- grad_b_proj: bfloat16 [2048, 1024], P('sp', 'tp')
- grad_c_proj: bfloat16 [2048, 1024], P('sp', 'tp')
- grad_log_decay: float32 [2048, 32], P('sp', 'tp')
Inputs may be any that keep to these rules, and one draw needn't show every extreme that they name: `expert_choice`: in the 128 rows of one device no expert is named more than 32 times, a bound that some blocks reach; the 2 entries of a row differ.
All inputs are finite; a program needn't handle non-finite values.
Results may differ from a plain program's by a relative error of at most 0.012.
Values may be sent and summed in bfloat16 or wider, within the bound.
A program may use at most 192 MiB of HBM per device.

v0:
```python
import jax
import jax.numpy as jnp
from jax import lax
from jax.sharding import PartitionSpec as P

HEAD_DIM = 64
STATE = 128
rms_epsilon = 1e-05
clamp_limit = 7.0
swish_alpha = 1.702


def entry_slots(expert_choice, expert_count, capacity):
    tokens, top_count = expert_choice.shape
    targets = expert_choice.reshape(-1)
    experts = jnp.arange(expert_count, dtype=jnp.int32)
    one_hot = (targets[:, None] == experts[None, :]).astype(jnp.float32)
    entries = jnp.arange(tokens * top_count, dtype=jnp.int32)
    before = (entries[:, None] > entries[None, :]).astype(jnp.bfloat16)
    earlier = jnp.dot(before, one_hot.astype(jnp.bfloat16), preferred_element_type=jnp.float32)
    ranks = jnp.sum(earlier * one_hot, axis=1).astype(jnp.int32)
    return (targets * capacity + ranks).reshape(tokens, top_count)


def expert_side(grad_rows, gate_value, up_value, gate_weight, up_weight, down_weight):
    act_grad = jnp.einsum("rd,fd->rf", grad_rows, down_weight, preferred_element_type=jnp.float32)
    gate_full = gate_value.astype(jnp.float32)
    up_full = up_value.astype(jnp.float32)
    gate_clip = jnp.minimum(gate_full, clamp_limit)
    up_clip = jnp.clip(up_full, -clamp_limit, clamp_limit)
    sigmoid_gate = jax.nn.sigmoid(swish_alpha * gate_clip)
    swish_gate = gate_clip * sigmoid_gate
    active = ((up_clip + 1.0) * swish_gate).astype(jnp.bfloat16)
    up_grad = jnp.where(
        (up_full > -clamp_limit) & (up_full < clamp_limit), act_grad * swish_gate, 0.0
    ).astype(jnp.bfloat16)
    slope = sigmoid_gate + swish_alpha * gate_clip * sigmoid_gate * (1.0 - sigmoid_gate)
    gate_grad = jnp.where(gate_full < clamp_limit, act_grad * (up_clip + 1.0) * slope, 0.0).astype(
        jnp.bfloat16
    )
    partial_rows = jnp.einsum(
        "rf,df->rd", gate_grad, gate_weight, preferred_element_type=jnp.float32
    )
    partial_rows = partial_rows + jnp.einsum(
        "rf,df->rd", up_grad, up_weight, preferred_element_type=jnp.float32
    )
    return (active, gate_grad, up_grad, partial_rows)


def exchange(pieces):
    return lax.all_to_all(pieces, "sp", split_axis=0, concat_axis=0, tiled=True)


def tell_all(vector):
    return exchange(jnp.broadcast_to(vector, (lax.axis_size("sp"), *vector.shape)))


def later_states(block_state, totals):
    count = lax.axis_size("sp")
    heads, channels, width = block_state.shape
    rows = heads * channels // count
    spots = jnp.arange(count)
    between = (
        (spots[:, None, None] < spots[None, None, :])
        & (spots[None, None, :] < spots[None, :, None])
    ).astype(jnp.float32)
    gaps = jnp.einsum("bck,kh->bch", between, totals, precision=lax.Precision.HIGHEST)
    later = spots[:, None, None] < spots[None, :, None]
    weights = jnp.where(later, jnp.exp(gaps), 0.0)
    first = lax.axis_index("sp") * rows
    picks = (
        ((first + jnp.arange(rows)) // channels)[None, :] == jnp.arange(heads)[:, None]
    ).astype(jnp.float32)
    weights = jnp.einsum("bch,hr->bcr", weights, picks, precision=lax.Precision.HIGHEST)
    dealt = lax.all_to_all(
        block_state.astype(jnp.bfloat16).reshape(count, rows, width),
        "sp",
        split_axis=0,
        concat_axis=0,
        tiled=True,
    ).astype(jnp.float32)
    sums = jnp.sum(weights[:, :, :, None] * dealt[None], axis=1)
    back = lax.all_to_all(sums.astype(jnp.bfloat16), "sp", split_axis=0, concat_axis=0, tiled=True)
    return back.reshape(heads, channels, width)


def body(
    mixer_output,
    layer_cotangent,
    expert_choice,
    route_weight,
    gate_pre,
    up_pre,
    w_gate,
    w_up,
    w_down,
    w_out,
    norm_gain,
    scan_in,
    gate_in,
    b_proj,
    c_proj,
    log_decay,
    entry_state,
):
    expert_count = lax.axis_size("sp")
    tokens_here = mixer_output.shape[0]
    model_width = mixer_output.shape[1]
    top_count = expert_choice.shape[1]
    capacity = gate_pre.shape[1] // expert_count
    columns = model_width // lax.axis_size("tp")
    first_column = lax.axis_index("tp") * columns
    own_cotangent = lax.dynamic_slice_in_dim(layer_cotangent, first_column, columns, 1).astype(
        jnp.float32
    )
    own_hidden = lax.dynamic_slice_in_dim(mixer_output, first_column, columns, 1)
    slots = entry_slots(expert_choice, expert_count, capacity)
    slot_ids = jnp.arange(expert_count * capacity, dtype=jnp.int32)
    places = (slots.T[:, None, :] == slot_ids[None, :, None]).astype(jnp.bfloat16)
    token_places = places.sum(axis=0)
    weighted = (route_weight.T[:, :, None] * own_cotangent[None]).astype(jnp.bfloat16)

    def dispatch(rows):
        arrived = lax.all_to_all(
            rows.astype(jnp.bfloat16).reshape(expert_count, capacity, columns),
            "sp",
            split_axis=0,
            concat_axis=0,
            tiled=True,
        ).reshape(-1, columns)
        return lax.all_gather(arrived, "tp", axis=1, tiled=True)

    recv_grads = dispatch(
        jnp.einsum("kst,ktd->sd", places, weighted, preferred_element_type=jnp.float32)
    )
    active, gate_grad, up_grad, partial_rows = expert_side(
        recv_grads, gate_pre[0], up_pre[0], w_gate[0], w_up[0], w_down[0]
    )
    summed = lax.psum_scatter(
        partial_rows.astype(jnp.bfloat16), "tp", scatter_dimension=1, tiled=True
    )
    returned = lax.all_to_all(
        summed.reshape(expert_count, capacity, -1), "sp", split_axis=0, concat_axis=0, tiled=True
    )
    head_count = log_decay.shape[1]
    group_count = b_proj.shape[1] // STATE
    per_group = head_count // group_count
    scan_heads = scan_in.reshape(tokens_here, head_count, HEAD_DIM)
    b_groups = b_proj.reshape(tokens_here, group_count, STATE)
    c_groups = c_proj.reshape(tokens_here, group_count, STATE)
    x_float = scan_heads.astype(jnp.float32)
    token_locations = jnp.arange(tokens_here)
    causal = token_locations[:, None] >= token_locations[None, :]
    causal_float = causal.astype(jnp.float32)
    cumulative = jnp.dot(causal_float, log_decay, precision=lax.Precision.HIGHEST)
    growth = jnp.exp(cumulative)
    block_decays = tell_all(lax.optimization_barrier((cumulative[-1], summed))[0])
    tail_decay = jnp.exp(cumulative[-1][None, :] - cumulative)
    log_gaps = cumulative.T[:, :, None] - cumulative.T[:, None, :]
    decay_mat = jnp.exp(jnp.where(causal[None], log_gaps, -jnp.inf))
    inner_prod = jnp.einsum("tgn,sgn->gts", c_groups, b_groups, preferred_element_type=jnp.float32)
    mix_weights = (jnp.repeat(inner_prod, per_group, axis=0) * decay_mat).astype(jnp.bfloat16)
    state_groups = entry_state.astype(jnp.bfloat16).reshape(group_count, per_group, HEAD_DIM, STATE)
    y_inner = jnp.einsum(
        "hts,shp->thp", mix_weights, scan_heads, preferred_element_type=jnp.float32
    )
    y_carry = jnp.einsum(
        "tgn,grpn->tgrp", c_groups, state_groups, preferred_element_type=jnp.float32
    ).reshape(tokens_here, head_count, HEAD_DIM)
    scan_out = y_inner + y_carry * growth[:, :, None]
    gate_float = gate_in.astype(jnp.float32)
    gate_sig = jax.nn.sigmoid(gate_float)
    gate_silu = gate_float * gate_sig
    gated = scan_out.reshape(tokens_here, -1) * gate_silu
    grouped = gated.reshape(tokens_here, group_count, -1)
    inv_rms = lax.rsqrt(jnp.mean(grouped * grouped, axis=-1, keepdims=True) + rms_epsilon)
    unit = grouped * inv_rms
    gain_groups = norm_gain.astype(jnp.float32).reshape(group_count, -1)
    mixed = (unit * gain_groups).reshape(tokens_here, -1).astype(jnp.bfloat16)
    all_mixed = lax.all_gather(mixed, "sp", axis=0, tiled=True)
    returned, mixed = lax.optimization_barrier((returned, mixed))
    moe_terms = jnp.einsum(
        "st,sd->td", token_places, returned.reshape(-1, columns), preferred_element_type=jnp.float32
    )
    grad_hidden = lax.all_gather(
        (own_cotangent + moe_terms).astype(jnp.bfloat16), "tp", axis=1, tiled=True
    )
    late_hidden, grad_hidden = lax.optimization_barrier((own_hidden, grad_hidden))
    recv_hidden = dispatch(
        jnp.einsum("st,td->sd", token_places, late_hidden, preferred_element_type=jnp.float32)
    )
    down_wgrad = jnp.einsum(
        "rf,rd->fd", active, recv_grads, preferred_element_type=jnp.float32
    ).astype(jnp.bfloat16)
    gate_wgrad = jnp.einsum(
        "rd,rf->df", recv_hidden, gate_grad, preferred_element_type=jnp.float32
    ).astype(jnp.bfloat16)
    up_wgrad = jnp.einsum(
        "rd,rf->df", recv_hidden, up_grad, preferred_element_type=jnp.float32
    ).astype(jnp.bfloat16)
    own_block = lax.all_to_all(
        grad_hidden.reshape(tokens_here, expert_count, -1).transpose(1, 0, 2),
        "sp",
        split_axis=0,
        concat_axis=0,
        tiled=True,
    )
    grad_out_proj = jnp.einsum(
        "td,ti->di",
        own_block.reshape(-1, own_block.shape[2]),
        all_mixed,
        preferred_element_type=jnp.float32,
    )
    grad_mixed = jnp.einsum("td,id->ti", grad_hidden, w_out, preferred_element_type=jnp.float32)
    grad_unit = grad_mixed.reshape(tokens_here, group_count, -1) * gain_groups
    grad_grouped = inv_rms * (grad_unit - unit * jnp.mean(grad_unit * unit, axis=-1, keepdims=True))
    grad_gated = grad_grouped.reshape(tokens_here, -1)
    grad_gate_in = (
        grad_gated
        * scan_out.reshape(tokens_here, -1)
        * gate_sig
        * (1.0 + gate_float * (1.0 - gate_sig))
    ).astype(jnp.bfloat16)
    grad_y = (grad_gated * gate_silu).reshape(tokens_here, head_count, HEAD_DIM)
    grad_y_b = grad_y.astype(jnp.bfloat16)
    grad_x_inner = jnp.einsum(
        "hts,thp->shp", mix_weights, grad_y_b, preferred_element_type=jnp.float32
    )
    grad_weights = (
        jnp.einsum("thp,shp->hts", grad_y_b, scan_heads, preferred_element_type=jnp.float32)
        * decay_mat
    )
    grad_weights = (
        grad_weights.reshape(group_count, per_group, tokens_here, tokens_here)
        .sum(axis=1)
        .astype(jnp.bfloat16)
    )
    grad_c_inner = jnp.einsum(
        "gts,sgn->tgn", grad_weights, b_groups, preferred_element_type=jnp.float32
    )
    grad_b_inner = jnp.einsum(
        "gts,tgn->sgn", grad_weights, c_groups, preferred_element_type=jnp.float32
    )
    grown_grads = (
        (grad_y * growth[:, :, None])
        .astype(jnp.bfloat16)
        .reshape(tokens_here, group_count, per_group, HEAD_DIM)
    )
    grad_c_carry = jnp.einsum(
        "tgrp,grpn->tgn", grown_grads, state_groups, preferred_element_type=jnp.float32
    )
    block_state = jnp.einsum(
        "tgrp,tgn->grpn", grown_grads, c_groups, preferred_element_type=jnp.float32
    ).reshape(head_count, HEAD_DIM, STATE)
    x_tail = (
        (x_float * tail_decay[:, :, None])
        .astype(jnp.bfloat16)
        .reshape(tokens_here, group_count, per_group, HEAD_DIM)
    )
    later_state = later_states(block_state, block_decays)
    later_groups = later_state.reshape(group_count, per_group, HEAD_DIM, STATE)
    grad_x_carry = jnp.einsum(
        "sgn,grpn->sgrp", b_groups, later_groups, preferred_element_type=jnp.float32
    ).reshape(tokens_here, head_count, HEAD_DIM)
    grad_x = grad_x_inner + grad_x_carry * tail_decay[:, :, None]
    grad_b_carry = jnp.einsum(
        "sgrp,grpn->sgn", x_tail, later_groups, preferred_element_type=jnp.float32
    )
    grad_a = jnp.sum(grad_y * scan_out, axis=2) - jnp.sum(x_float * grad_x, axis=2)
    block_totals = tell_all(jnp.sum(grad_a, axis=0))
    is_later = jnp.arange(expert_count) > lax.axis_index("sp")
    later_grad = jnp.sum(jnp.where(is_later[:, None], block_totals, 0.0), axis=0)
    grad_log_decay = (
        jnp.dot(causal_float.T, grad_a, precision=lax.Precision.HIGHEST) + later_grad[None, :]
    )
    grad_scan_in = grad_x.reshape(tokens_here, -1).astype(jnp.bfloat16)
    grad_b_proj = (grad_b_inner + grad_b_carry).reshape(tokens_here, -1).astype(jnp.bfloat16)
    grad_c_proj = (grad_c_inner + grad_c_carry).reshape(tokens_here, -1).astype(jnp.bfloat16)
    return (
        gate_wgrad[None],
        up_wgrad[None],
        down_wgrad[None],
        grad_out_proj,
        grad_scan_in,
        grad_gate_in,
        grad_b_proj,
        grad_c_proj,
        grad_log_decay,
    )


def solution(mesh):
    in_specs = (
        P("sp", None),
        P("sp", None),
        P("sp", None),
        P("sp", None),
        P("sp", None, "tp"),
        P("sp", None, "tp"),
        P("sp", None, "tp"),
        P("sp", None, "tp"),
        P("sp", "tp", None),
        P("tp", None),
        P("tp"),
        P("sp", "tp"),
        P("sp", "tp"),
        P("sp", "tp"),
        P("sp", "tp"),
        P("sp", "tp"),
        P("sp", "tp", None, None),
    )
    out_specs = (
        P("sp", None, "tp"),
        P("sp", None, "tp"),
        P("sp", "tp", None),
        P("sp", "tp"),
        P("sp", "tp"),
        P("sp", "tp"),
        P("sp", "tp"),
        P("sp", "tp"),
        P("sp", "tp"),
    )
    return jax.shard_map(body, mesh=mesh, in_specs=in_specs, out_specs=out_specs, check_vma=False)
```

profile of v0, /device:TPU:0, one launch (start us, length us, event | category | flops | bytes accessed | tf_op | source)
XLA Modules:
  0.0 248.3 jit_solution(7997684214962049168)
XLA Ops:
  12.6 34.6 %all_to_all.48 = bf16[16,32,1024]{2,1,0:T(8,128)(2,1)} all-to-all(bf16[16,32,1024]{2,1,0:T(8,128)(2,1)S(1)} %bitcast.204), channel_id=1, replica_groups=mesh['sp'=16,'tp'=2] {'sp'}, dimensions={0} | all-to-all | bytes 2097152 | tf_op jit(solution)/shard_map/all_to_all | solution.py:124
  47.2 9.0 %all-gather.4.cloned.1.call-done = bf16[512,2048]{1,0:T(8,128)(2,1)} async-done(((bf16[512,1024]{1,0:T(8,128)(2,1)}), bf16[512,2048]{1,0:T(8,128)(2,1)}) %all-gather.4.cloned.1.call-update) | async-done | bytes 2097168 | tf_op jit(solution)/shard_map/all_gather | solution.py:131
  56.2 3.8 %select_convert_fusion = (bf16[512,512]{1,0:T(8,128)(2,1)S(1)}, f32[512,512]{1,0:T(8,128)S(1)}) fusion(bf16[1,512,512]{2,1,0:T(8,128)(2,1)S(1)} %copy-done.42, bf16[1,512,512]{2,1,0:T(8,128)(2,1)S(1)} %copy-done.40, bf16[512,2048]{1,0:T(8,128)(2,1)} %all-gather.4.cloned.1.call-done, bf16[1,512,2048]{2,1,0:T(8,128)(2,1)} %param.25), kind=kOutput, calls=%fused_computation.62 | convolution fusion | flops 1077411840 | bytes 6815744 | tf_op jit(solution)/shard_map/rd,fd->rf/dot_general | solution.py:26
  62.3 2.6 %add_convert_fusion = bf16[512,2048]{1,0:T(8,128)(2,1)} fusion(f32[512,2048]{1,0:T(8,128)S(1)} %fusion.4, bf16[512,512]{1,0:T(8,128)(2,1)S(1)} %get-tuple-element.79, bf16[1,2048,512]{2,1,0:T(8,128)(2,1)S(1)} %copy-done.11), kind=kOutput, calls=%fused_computation.1 | convolution fusion | flops 1075838976 | bytes 8912896 | tf_op jit(solution)/shard_map/rf,df->rd/dot_general | solution.py:44
  75.9 7.0 %all-to-all-start.1 = ((bf16[16,32,1024]{2,1,0:T(8,128)(2,1)}), bf16[16,32,1024]{2,1,0:T(8,128)(2,1)}, u32[]{:S(2)}, u32[]{:S(2)}) async-start(bf16[16,32,1024]{2,1,0:T(8,128)(2,1)} %bitcast.217), calls=%async_computation.2 | async-start | bytes 2097152 | tf_op jit(solution)/shard_map/all_to_all | solution.py:142
  85.2 27.8 %all-to-all-done.1 = bf16[16,32,1024]{2,1,0:T(8,128)(2,1)} async-done(((bf16[16,32,1024]{2,1,0:T(8,128)(2,1)}), bf16[16,32,1024]{2,1,0:T(8,128)(2,1)}, u32[]{:S(2)}, u32[]{:S(2)}) %all-to-all-start.1) | async-done | bytes 1048608 | tf_op jit(solution)/shard_map/all_to_all | solution.py:142
  113.7 6.2 %all-to-all-start.4 = ((f32[16,1,16]{2,1,0:T(1,128)}), f32[16,1,16]{2,1,0:T(1,128)}, u32[]{:S(2)}, u32[]{:S(2)}) async-start(f32[16,1,16]{2,1,0:T(1,128)} %broadcast_in_dim.61), calls=%async_computation.5 | async-start | bytes 16384 | tf_op jit(solution)/shard_map/all_to_all | solution.py:51
  124.5 4.5 %fusion.86 = f32[128,1024]{1,0:T(8,128)} fusion(bf16[128,2048]{1,0:T(8,128)(2,1)S(1)} %all_gather.13, bf16[1024,2048]{1,0:T(8,128)(2,1)} %param.26), kind=kOutput, calls=%fused_computation.145 | convolution fusion | flops 536870912 | bytes 5242880 | tf_op jit(solution)/shard_map/td,id->ti/dot_general | solution.py:214
  137.4 6.9 %all-to-all-start.5 = ((bf16[16,64,128]{2,1,0:T(8,128)(2,1)}), bf16[16,64,128]{2,1,0:T(8,128)(2,1)}, u32[]{:S(2)}, u32[]{:S(2)}) async-start(bf16[16,64,128]{2,1,0:T(8,128)(2,1)} %bitcast.216), calls=%async_computation.6 | async-start | bytes 524288 | tf_op jit(solution)/shard_map/all_to_all | solution.py:75
  144.3 2.4 convolution_convert_fusion.3
  146.7 12.2 %all-to-all-done.5 = bf16[16,64,128]{2,1,0:T(8,128)(2,1)} async-done(((bf16[16,64,128]{2,1,0:T(8,128)(2,1)}), bf16[16,64,128]{2,1,0:T(8,128)(2,1)}, u32[]{:S(2)}, u32[]{:S(2)}) %all-to-all-start.5) | async-done | bytes 262176 | tf_op jit(solution)/shard_map/all_to_all | solution.py:75
  158.9 7.2 %all-to-all-start.2 = ((bf16[16,32,1024]{2,1,0:T(8,128)(2,1)}), bf16[16,32,1024]{2,1,0:T(8,128)(2,1)}, u32[]{:S(2)}, u32[]{:S(2)}) async-start(bf16[16,32,1024]{2,1,0:T(8,128)(2,1)} %bitcast.202), calls=%async_computation.3 | async-start | bytes 2097152 | tf_op jit(solution)/shard_map/all_to_all | solution.py:124
  166.6 4.8 %fusion.2 = bf16[1,512,2048]{2,1,0:T(8,128)(2,1)} fusion(bf16[512,2048]{1,0:T(8,128)(2,1)} %all-gather.4.cloned.1.call-done, bf16[1,512,512]{2,1,0:T(8,128)(2,1)} %param.22, bf16[1,512,512]{2,1,0:T(8,128)(2,1)} %param.21), kind=kOutput, calls=%fused_computation.7 | convolution fusion | flops 1077936128 | bytes 5242880 | tf_op jit(solution)/shard_map/rf,rd->fd/dot_general | solution.py:192
  175.7 3.3 %multiply_reduce_fusion = bf16[16,64,128]{2,1,0:T(8,128)(2,1)} fusion(f32[16,64,128]{2,1,0:T(8,128)S(1)} %convert_element_type.168, f32[16,16,64]{2,1,0:T(8,128)S(1)} %fusion.74), kind=kLoop, calls=%fused_computation | loop fusion | flops 4063232 | bytes 851968 | tf_op jit(solution)/shard_map/reduce_sum | solution.py:82
  179.0 10.2 %all-to-all-done.2 = bf16[16,32,1024]{2,1,0:T(8,128)(2,1)} async-done(((bf16[16,32,1024]{2,1,0:T(8,128)(2,1)}), bf16[16,32,1024]{2,1,0:T(8,128)(2,1)}, u32[]{:S(2)}, u32[]{:S(2)}) %all-to-all-start.2) | async-done | bytes 1048608 | tf_op jit(solution)/shard_map/all_to_all | solution.py:124
  189.2 6.0 %all-to-all-start.6 = ((bf16[16,64,128]{2,1,0:T(8,128)(2,1)}), bf16[16,64,128]{2,1,0:T(8,128)(2,1)}, u32[]{:S(2)}, u32[]{:S(2)}) async-start(bf16[16,64,128]{2,1,0:T(8,128)(2,1)} %multiply_reduce_fusion), calls=%async_computation.7 | async-start | bytes 524288 | tf_op jit(solution)/shard_map/all_to_all | solution.py:83
  200.9 2.8 %all-to-all-done.6 = bf16[16,64,128]{2,1,0:T(8,128)(2,1)} async-done(((bf16[16,64,128]{2,1,0:T(8,128)(2,1)}), bf16[16,64,128]{2,1,0:T(8,128)(2,1)}, u32[]{:S(2)}, u32[]{:S(2)}) %all-to-all-start.6) | async-done | bytes 262176 | tf_op jit(solution)/shard_map/all_to_all | solution.py:83
  203.8 4.2 %all-to-all-start.3 = ((bf16[16,128,128]{2,1,0:T(8,128)(2,1)}), bf16[16,128,128]{2,1,0:T(8,128)(2,1)}, u32[]{:S(2)}, u32[]{:S(2)}) async-start(bf16[16,128,128]{2,1,0:T(8,128)(2,1)} %bitcast_bitcast_fusion), calls=%async_computation.4 | async-start | bytes 1048576 | tf_op jit(solution)/shard_map/all_to_all | solution.py:201
  217.0 4.0 %all-to-all-done.3 = bf16[16,128,128]{2,1,0:T(8,128)(2,1)} async-done(((bf16[16,128,128]{2,1,0:T(8,128)(2,1)}), bf16[16,128,128]{2,1,0:T(8,128)(2,1)}, u32[]{:S(2)}, u32[]{:S(2)}) %all-to-all-start.3) | async-done | bytes 524320 | tf_op jit(solution)/shard_map/all_to_all | solution.py:201
  221.6 3.8 %all-to-all-start.7 = ((f32[16,1,16]{2,1,0:T(1,128)}), f32[16,1,16]{2,1,0:T(1,128)S(1)}, u32[]{:S(2)}, u32[]{:S(2)}) async-start(f32[16,1,16]{2,1,0:T(1,128)} %broadcast_in_dim.100), calls=%async_computation.8 | async-start | bytes 16384 | tf_op jit(solution)/shard_map/all_to_all | solution.py:51
  225.5 3.9 %fusion.85 = f32[128,1024]{1,0:T(8,128)} fusion(bf16[2048,128]{1,0:T(8,128)(2,1)} %bitcast.29, bf16[2048,1024]{1,0:T(8,128)(2,1)} %all-gather.8.cloned.1.call-done), kind=kOutput, calls=%fused_computation.144 | convolution fusion | flops 536870912 | bytes 5242880 | tf_op jit(solution)/shard_map/td,ti->di/dot_general | solution.py:208
  229.5 3.2 %all-to-all-done.7 = f32[16,1,16]{2,1,0:T(1,128)S(1)} async-done(((f32[16,1,16]{2,1,0:T(1,128)}), f32[16,1,16]{2,1,0:T(1,128)S(1)}, u32[]{:S(2)}, u32[]{:S(2)}) %all-to-all-start.7) | async-done | bytes 1056 | tf_op jit(solution)/shard_map/all_to_all | solution.py:51
  233.6 4.4 %fusion.1 = bf16[1,2048,512]{2,1,0:T(8,128)(2,1)} fusion(bf16[512,2048]{1,0:T(8,128)(2,1)} %all-gather.6.cloned.1.call-done, bf16[512,512]{1,0:T(8,128)(2,1)S(1)} %copy-done.21), kind=kOutput, calls=%fused_computation.6 | convolution fusion | flops 1074790400 | bytes 4718592 | tf_op jit(solution)/shard_map/rd,rf->df/dot_general | solution.py:198
  238.0 2.9 %fusion = bf16[1,2048,512]{2,1,0:T(8,128)(2,1)} fusion(bf16[512,2048]{1,0:T(8,128)(2,1)S(1)} %copy-done.39, bf16[1,512,512]{2,1,0:T(8,128)(2,1)S(1)} %copy-done.41, f32[512,512]{1,0:T(8,128)S(1)} %copy-done.45, bf16[1,512,512]{2,1,0:T(8,128)(2,1)S(1)} %copy-done.43), kind=kOutput, calls=%fused_computation.5 | convolution fusion | flops 1079508992 | bytes 6291456 | tf_op jit(solution)/shard_map/rd,rf->df/dot_general | solution.py:195
  (176 shorter events, 54.2 us)
Async XLA Ops:
  8.0 52.1 %copy-start = (bf16[1,2048,512]{2,1,0:T(8,128)(2,1)S(1)}, bf16[1,2048,512]{2,1,0:T(8,128)(2,1)}, u32[]{:S(2)}) copy-start(bf16[1,2048,512]{2,1,0:T(8,128)(2,1)} %param.23) | copy-start | bytes 6291460
  8.0 48.2 %all-gather.4.cloned.1.call-start = ((), (), s32[]{:S(2)}) async-start(), calls=%async_computation.9 | async-start | bytes 3145728 | tf_op jit(solution)/shard_map/all_gather | solution.py:131
  10.3 36.9 %copy-start.31 = (s32[2,128]{1,0:T(2,128)}, s32[2,128]{1,0:T(2,128)S(1)}, u32[]{:S(2)}) copy-start(s32[2,128]{1,0:T(2,128)S(1)} %add_bitcast_fusion) | copy-start | bytes 3076
  11.3 45.0 %copy-start.40 = (bf16[1,512,512]{2,1,0:T(8,128)(2,1)S(1)}, bf16[1,512,512]{2,1,0:T(8,128)(2,1)}, u32[]{:S(2)}) copy-start(bf16[1,512,512]{2,1,0:T(8,128)(2,1)} %param.21) | copy-start | bytes 1572868
  11.3 45.0 %copy-start.42 = (bf16[1,512,512]{2,1,0:T(8,128)(2,1)S(1)}, bf16[1,512,512]{2,1,0:T(8,128)(2,1)}, u32[]{:S(2)}) copy-start(bf16[1,512,512]{2,1,0:T(8,128)(2,1)} %param.22) | copy-start | bytes 1572868
  47.2 28.7 %reduce-scatter.2.cloned.1.call-start = ((), (), s32[]{:S(2)}) async-start(), calls=%async_computation.10 | async-start | bytes 3145728 | tf_op jit(solution)/shard_map/reduce_scatter | solution.py:139
  64.9 160.6 %all-gather.8.cloned.1.call-start = ((), (), s32[]{:S(2)}) async-start(), calls=%async_computation.12 | async-start | bytes 4456448 | tf_op jit(solution)/shard_map/all_gather | solution.py:180
  75.5 7.4 %copy-start.34 = (bf16[1024]{0:T(1024)(128)(2,1)S(1)}, bf16[1024]{0:T(1024)(128)(2,1)}, u32[]{:S(2)}) copy-start(bf16[1024]{0:T(1024)(128)(2,1)} %param.27) | copy-start | bytes 6148
  75.5 8.0 %copy-start.32 = (s32[2,128]{1,0:T(2,128)S(1)}, s32[2,128]{1,0:T(2,128)}, u32[]{:S(2)}) copy-start(s32[2,128]{1,0:T(2,128)} %copy-done.31) | copy-start | bytes 3076
  75.5 37.6 %copy-start.37 = (f32[16]{0:T(128)S(1)}, f32[16]{0:T(128)}, u32[]{:S(2)}) copy-start(f32[16]{0:T(128)} %copy-done.36) | copy-start | bytes 196
  75.9 37.2 %all-to-all-start.1 = ((bf16[16,32,1024]{2,1,0:T(8,128)(2,1)}), bf16[16,32,1024]{2,1,0:T(8,128)(2,1)}, u32[]{:S(2)}, u32[]{:S(2)}) async-start(bf16[16,32,1024]{2,1,0:T(8,128)(2,1)} %bitcast.217), calls=%async_computation.2 | async-start | bytes 2097152 | tf_op jit(solution)/shard_map/all_to_all | solution.py:142
  83.5 40.2 %copy-start.18 = (bf16[512,128]{1,0:T(8,128)(2,1)}, bf16[512,128]{1,0:T(8,128)(2,1)S(1)}, u32[]{:S(2)}) copy-start(bf16[512,128]{1,0:T(8,128)(2,1)S(1)} %fusion.52) | copy-start | bytes 393220
  113.7 23.7 %all-to-all-start.4 = ((f32[16,1,16]{2,1,0:T(1,128)}), f32[16,1,16]{2,1,0:T(1,128)}, u32[]{:S(2)}, u32[]{:S(2)}) async-start(f32[16,1,16]{2,1,0:T(1,128)} %broadcast_in_dim.61), calls=%async_computation.5 | async-start | bytes 16384 | tf_op jit(solution)/shard_map/all_to_all | solution.py:51
  137.4 21.5 %all-to-all-start.5 = ((bf16[16,64,128]{2,1,0:T(8,128)(2,1)}), bf16[16,64,128]{2,1,0:T(8,128)(2,1)}, u32[]{:S(2)}, u32[]{:S(2)}) async-start(bf16[16,64,128]{2,1,0:T(8,128)(2,1)} %bitcast.216), calls=%async_computation.6 | async-start | bytes 524288 | tf_op jit(solution)/shard_map/all_to_all | solution.py:75
  158.9 30.3 %all-to-all-start.2 = ((bf16[16,32,1024]{2,1,0:T(8,128)(2,1)}), bf16[16,32,1024]{2,1,0:T(8,128)(2,1)}, u32[]{:S(2)}, u32[]{:S(2)}) async-start(bf16[16,32,1024]{2,1,0:T(8,128)(2,1)} %bitcast.202), calls=%async_computation.3 | async-start | bytes 2097152 | tf_op jit(solution)/shard_map/all_to_all | solution.py:124
  173.6 21.7 %copy-start.17 = (bf16[128,4,128]{0,2,1:T(8,128)(2,1)S(1)}, bf16[128,4,128]{0,2,1:T(8,128)(2,1)}, u32[]{:S(2)}) copy-start(bf16[128,4,128]{0,2,1:T(8,128)(2,1)} %copy-done.16) | copy-start | bytes 393220
  189.2 14.6 %all-to-all-start.6 = ((bf16[16,64,128]{2,1,0:T(8,128)(2,1)}), bf16[16,64,128]{2,1,0:T(8,128)(2,1)}, u32[]{:S(2)}, u32[]{:S(2)}) async-start(bf16[16,64,128]{2,1,0:T(8,128)(2,1)} %multiply_reduce_fusion), calls=%async_computation.7 | async-start | bytes 524288 | tf_op jit(solution)/shard_map/all_to_all | solution.py:83
  195.2 38.3 %all-gather.6.cloned.1.call-start = ((), (), s32[]{:S(2)}) async-start(), calls=%async_computation.11 | async-start | bytes 3145728 | tf_op jit(solution)/shard_map/all_gather | solution.py:131
  198.8 9.2 %copy-start.26 = (f32[128,16]{0,1:T(8,128)S(1)}, f32[128,16]{0,1:T(8,128)}, u32[]{:S(2)}) copy-start(f32[128,16]{0,1:T(8,128)} %get-tuple-element.77) | copy-start | bytes 24580
  200.9 12.0 %copy-start.14 = (bf16[128,4,128]{2,1,0:T(4,128)(2,1)S(1)}, bf16[128,4,128]{2,1,0:T(4,128)(2,1)}, u32[]{:S(2)}) copy-start(bf16[128,4,128]{2,1,0:T(4,128)(2,1)} %copy-done.13) | copy-start | bytes 393220
  203.8 17.2 %all-to-all-start.3 = ((bf16[16,128,128]{2,1,0:T(8,128)(2,1)}), bf16[16,128,128]{2,1,0:T(8,128)(2,1)}, u32[]{:S(2)}, u32[]{:S(2)}) async-start(bf16[16,128,128]{2,1,0:T(8,128)(2,1)} %bitcast_bitcast_fusion), calls=%async_computation.4 | async-start | bytes 1048576 | tf_op jit(solution)/shard_map/all_to_all | solution.py:201
  221.6 11.1 %all-to-all-start.7 = ((f32[16,1,16]{2,1,0:T(1,128)}), f32[16,1,16]{2,1,0:T(1,128)S(1)}, u32[]{:S(2)}, u32[]{:S(2)}) async-start(f32[16,1,16]{2,1,0:T(1,128)} %broadcast_in_dim.100), calls=%async_computation.8 | async-start | bytes 16384 | tf_op jit(solution)/shard_map/all_to_all | solution.py:51
  225.5 7.2 %copy-start.38 = (pred[16]{0:T(512)(128)(4,1)S(1)}, pred[16]{0:T(512)(128)(4,1)}, u32[]{:S(2)}) copy-start(pred[16]{0:T(512)(128)(4,1)} %iota_compare_fusion.11) | copy-start | bytes 52
  225.5 8.0 %copy-start.21 = (bf16[512,512]{1,0:T(8,128)(2,1)S(1)}, bf16[512,512]{1,0:T(8,128)(2,1)}, u32[]{:S(2)}) copy-start(bf16[512,512]{1,0:T(8,128)(2,1)} %copy-done.20) | copy-start | bytes 1572868
  (33 other events, 82.5 us)
Sparse Core Ops, SparseCore 0:
  47.3 8.8 all-gather.3
  65.0 10.7 reduce-scatter.1
Sparse Core Ops, SparseCore 1:
  75.6 89.1 all-gather.7
  200.9 11.7 all-gather.5
where the time goes:
time: 250 us; the launch traced here: 248 us
  waiting for transfers between devices  69.7 us (28%)
  matrix products  47.4 us (19%)
  starting transfers between devices  41.5 us (17%)
  blocking collectives  36.7 us (15%)
  local copies, waits for them, and re-layouts  21.3 us (9%)
  between operations  16.3 us (7%)
  other arithmetic  15.4 us (6%)
    all_to_all x1, blocking collectives, dispatch(): lax.all_to_all(rows.astype(jnp.bfloat16).reshape(expert_count, capacity,...  34.6 us
    all_to_all x1, waiting for transfers between devices, body(): lax.all_to_all(summed.reshape(expert_count, capacity, -1), 'sp', split_ax...  27.8 us
    all_to_all x1, waiting for transfers between devices, later_states(): lax.all_to_all(block_state.astype(jnp.bfloat16).reshape(count, rows, widt...  12.2 us
    all_to_all x1, waiting for transfers between devices, dispatch(): lax.all_to_all(rows.astype(jnp.bfloat16).reshape(expert_count, capacity,...  10.2 us
    all_to_all x2, starting transfers between devices, exchange(): return lax.all_to_all(pieces, 'sp', split_axis=0, concat_axis=0, tiled=True)  10.1 us
    unnamed x99, local copies, waits for them, and re-layouts  9.1 us
    all_gather x2, waiting for transfers between devices, dispatch(): return lax.all_gather(arrived, 'tp', axis=1, tiled=True)  9.01 us
    all_to_all x1, starting transfers between devices, dispatch(): lax.all_to_all(rows.astype(jnp.bfloat16).reshape(expert_count, capacity,...  7.18 us
  transfers between devices with their start and end apart: 11, of which 8 were waited for; matrix products, arithmetic and copies ran while one was open for 25% of the time, Pallas kernels for 0%

commit v1 on v0

--- a/solution.py
+++ b/solution.py
@@ -128,7 +128,20 @@
             concat_axis=0,
             tiled=True,
         ).reshape(-1, columns)
-        return lax.all_gather(arrived, "tp", axis=1, tiled=True)
+
+        def _edit_roots(arr):
+            view_out = jnp.concatenate(
+                jax.lax.all_to_all(
+                    jnp.stack([arr] * jax.lax.axis_size("tp")),
+                    concat_axis=0,
+                    axis_name="tp",
+                    split_axis=0,
+                ),
+                1,
+            )
+            return view_out
+
+        return _edit_roots(arrived)
 
     recv_grads = dispatch(
         jnp.einsum("kst,ktd->sd", places, weighted, preferred_element_type=jnp.float32)

time: 250 us -> 259 us (1.036)
  blocking collectives: 36.7 us -> 49.5 us
  matrix products: 47.4 us -> 39.3 us
  waiting for transfers between devices: 69.7 us -> 76.8 us
  starting transfers between devices: 41.5 us -> 38.2 us
    all_to_all x0 -> x2, blocking collectives: none -> 12.6 us  [_edit_roots(): jax.lax.all_to_all(jnp.stack([arr] * jax.lax.axis_size('tp')), concat_axi...]
    all_to_all x1, waiting for transfers between devices: 4.01 us -> 13.3 us  [body(): lax.all_to_all(grad_hidden.reshape(tokens_here, expert_count, -1).transpo...]
    all_gather x2 -> x0, waiting for transfers between devices: 9.01 us -> none  [dispatch(): return lax.all_gather(arrived, 'tp', axis=1, tiled=True)]
    all_to_all x1, waiting for transfers between devices: 2.84 us -> 9.82 us  [later_states(): lax.all_to_all(sums.astype(jnp.bfloat16), 'sp', split_axis=0, concat_axis...]
    reshape x0 -> x2, local copies, waits for them, and re-layouts: none -> 6.94 us  [_edit_roots(): jnp.concatenate(jax.lax.all_to_all(jnp.stack([arr] * jax.lax.axis_size('t...]
    all_to_all x1, starting transfers between devices: 7.18 us -> 3.66 us  [dispatch(): lax.all_to_all(rows.astype(jnp.bfloat16).reshape(expert_count, capacity,...]
    all_to_all x1, waiting for transfers between devices: 27.8 us -> 25.1 us  [body(): lax.all_to_all(summed.reshape(expert_count, capacity, -1), 'sp', split_ax...]
    unnamed x99 -> x117, local copies, waits for them, and re-layouts: 9.1 us -> 7.99 us
  transfers between devices with their start and end apart: 11 -> 9, of which waited for: 8 -> 7; matrix products, arithmetic and copies ran while one was open for 25% -> 18% of each run, Pallas kernels for 0% -> 0%
where the time goes in v1:
time: 259 us; the launch traced here: 257 us
  waiting for transfers between devices  76.8 us (30%)
  blocking collectives  49.5 us (19%)
  matrix products  39.3 us (15%)
  starting transfers between devices  38.2 us (15%)
  local copies, waits for them, and re-layouts  22.7 us (9%)
  between operations  16.3 us (6%)
  other arithmetic  14.7 us (6%)
    all_to_all x1, blocking collectives, dispatch(): lax.all_to_all(rows.astype(jnp.bfloat16).reshape(expert_count, capacity,...  34.5 us
    all_to_all x1, waiting for transfers between devices, body(): lax.all_to_all(summed.reshape(expert_count, capacity, -1), 'sp', split_ax...  25.1 us
    all_to_all x1, waiting for transfers between devices, later_states(): lax.all_to_all(block_state.astype(jnp.bfloat16).reshape(count, rows, widt...  13.6 us
    all_to_all x1, waiting for transfers between devices, body(): lax.all_to_all(grad_hidden.reshape(tokens_here, expert_count, -1).transpo...  13.3 us
    all_to_all x2, blocking collectives, _edit_roots(): jax.lax.all_to_all(jnp.stack([arr] * jax.lax.axis_size('tp')), concat_axi...  12.6 us
    all_to_all x2, starting transfers between devices, exchange(): return lax.all_to_all(pieces, 'sp', split_axis=0, concat_axis=0, tiled=True)  10 us
    all_to_all x1, waiting for transfers between devices, later_states(): lax.all_to_all(sums.astype(jnp.bfloat16), 'sp', split_axis=0, concat_axis...  9.82 us
    all_to_all x1, waiting for transfers between devices, dispatch(): lax.all_to_all(rows.astype(jnp.bfloat16).reshape(expert_count, capacity,...  9.22 us
  transfers between devices with their start and end apart: 9, of which 7 were waited for; matrix products, arithmetic and copies ran while one was open for 18% of the time, Pallas kernels for 0%

profile of v1, /device:TPU:0, one launch (start us, length us, event | category | flops | bytes accessed | tf_op | source)
XLA Modules:
  0.0 257.5 jit_solution(9731911924186246986)
XLA Ops:
  12.5 34.5 %all_to_all.58 = bf16[16,32,1024]{2,1,0:T(8,128)(2,1)S(1)} all-to-all(bf16[16,32,1024]{2,1,0:T(8,128)(2,1)S(1)} %bitcast.209), channel_id=1, replica_groups=mesh['sp'=16,'tp'=2] {'sp'}, dimensions={0} | all-to-all | bytes 2097152 | tf_op jit(solution)/shard_map/all_to_all | solution.py:124
  47.1 6.3 %all_to_all.59 = bf16[2,512,1024]{2,1,0:T(8,128)(2,1)} all-to-all(bf16[2,512,1024]{2,1,0:T(8,128)(2,1)S(1)} %pad_maximum_fusion), channel_id=1, replica_groups=mesh['sp'=16,'tp'=2] {'tp'}, dimensions={0} | all-to-all | bytes 4194304 | tf_op jit(solution)/shard_map/all_to_all | solution.py:134
  53.4 4.0 %copy.136 = bf16[512,2,1024]{0,2,1:T(8,128)(2,1)} copy(bf16[512,2,1024]{2,0,1:T(8,128)(2,1)} %bitcast.202) | data formatting | bytes 4194304 | tf_op jit(solution)/shard_map/reshape | solution.py:133
  57.5 3.8 %fusion.33 = (bf16[512,512]{1,0:T(8,128)(2,1)S(1)}, f32[512,512]{1,0:T(8,128)S(1)}) fusion(bf16[1,512,512]{2,1,0:T(8,128)(2,1)S(1)} %copy-done.47, bf16[1,512,512]{2,1,0:T(8,128)(2,1)S(1)} %copy-done.50, bf16[512,2048]{0,1:T(8,128)(2,1)} %bitcast.220, bf16[1,512,2048]{2,1,0:T(8,128)(2,1)} %param.25), kind=kOutput, calls=%fused_computation.59 | convolution fusion | flops 1077411840 | bytes 6815744 | tf_op jit(solution)/shard_map/rd,fd->rf/dot_general | solution.py:26
  74.3 7.1 %all-to-all-start.2 = ((bf16[16,32,1024]{2,1,0:T(8,128)(2,1)}), bf16[16,32,1024]{2,1,0:T(8,128)(2,1)}, u32[]{:S(2)}, u32[]{:S(2)}) async-start(bf16[16,32,1024]{2,1,0:T(8,128)(2,1)} %bitcast.228), calls=%async_computation.3 | async-start | bytes 2097152 | tf_op jit(solution)/shard_map/all_to_all | solution.py:155
  86.5 25.1 %all-to-all-done.2 = bf16[16,32,1024]{2,1,0:T(8,128)(2,1)} async-done(((bf16[16,32,1024]{2,1,0:T(8,128)(2,1)}), bf16[16,32,1024]{2,1,0:T(8,128)(2,1)}, u32[]{:S(2)}, u32[]{:S(2)}) %all-to-all-start.2) | async-done | bytes 1048608 | tf_op jit(solution)/shard_map/all_to_all | solution.py:155
  112.9 6.1 %all-to-all-start.6 = ((f32[16,1,16]{2,1,0:T(1,128)}), f32[16,1,16]{2,1,0:T(1,128)}, u32[]{:S(2)}, u32[]{:S(2)}) async-start(f32[16,1,16]{2,1,0:T(1,128)} %broadcast_in_dim.61), calls=%async_computation.7 | async-start | bytes 16384 | tf_op jit(solution)/shard_map/all_to_all | solution.py:51
  122.9 3.7 %fusion.95 = f32[128,1024]{1,0:T(8,128)S(1)} fusion(bf16[128,2048]{1,0:T(8,128)(2,1)S(1)} %all_gather.6, bf16[1024,2048]{1,0:T(8,128)(2,1)} %param.26), kind=kOutput, calls=%fused_computation.156 | convolution fusion | flops 536870912 | bytes 5242880 | tf_op jit(solution)/shard_map/td,id->ti/dot_general | solution.py:227
  131.9 6.9 %all-to-all-start.7 = ((bf16[16,64,128]{2,1,0:T(8,128)(2,1)}), bf16[16,64,128]{2,1,0:T(8,128)(2,1)S(1)}, u32[]{:S(2)}, u32[]{:S(2)}) async-start(bf16[16,64,128]{2,1,0:T(8,128)(2,1)} %bitcast.43), calls=%async_computation.8 | async-start | bytes 524288 | tf_op jit(solution)/shard_map/all_to_all | solution.py:75
  139.9 13.6 %all-to-all-done.7 = bf16[16,64,128]{2,1,0:T(8,128)(2,1)S(1)} async-done(((bf16[16,64,128]{2,1,0:T(8,128)(2,1)}), bf16[16,64,128]{2,1,0:T(8,128)(2,1)S(1)}, u32[]{:S(2)}, u32[]{:S(2)}) %all-to-all-start.7) | async-done | bytes 262176 | tf_op jit(solution)/shard_map/all_to_all | solution.py:75
  153.6 3.3 %multiply_reduce_fusion = bf16[16,64,128]{2,1,0:T(8,128)(2,1)} fusion(f32[16,64,128]{2,1,0:T(8,128)S(1)} %convert_element_type.174, f32[16,16,64]{2,1,0:T(8,128)S(1)} %fusion.83), kind=kLoop, calls=%fused_computation | loop fusion | flops 4063232 | bytes 851968 | tf_op jit(solution)/shard_map/reduce_sum | solution.py:82
  156.8 6.9 %all-to-all-start.8 = ((bf16[16,64,128]{2,1,0:T(8,128)(2,1)}), bf16[16,64,128]{2,1,0:T(8,128)(2,1)S(1)}, u32[]{:S(2)}, u32[]{:S(2)}) async-start(bf16[16,64,128]{2,1,0:T(8,128)(2,1)} %multiply_reduce_fusion), calls=%async_computation.9 | async-start | bytes 524288 | tf_op jit(solution)/shard_map/all_to_all | solution.py:83
  165.3 9.8 %all-to-all-done.8 = bf16[16,64,128]{2,1,0:T(8,128)(2,1)S(1)} async-done(((bf16[16,64,128]{2,1,0:T(8,128)(2,1)}), bf16[16,64,128]{2,1,0:T(8,128)(2,1)S(1)}, u32[]{:S(2)}, u32[]{:S(2)}) %all-to-all-start.8) | async-done | bytes 262176 | tf_op jit(solution)/shard_map/all_to_all | solution.py:83
  175.1 3.6 %all-to-all-start.5 = ((bf16[16,128,128]{2,1,0:T(8,128)(2,1)}), bf16[16,128,128]{2,1,0:T(8,128)(2,1)S(1)}, u32[]{:S(2)}, u32[]{:S(2)}) async-start(bf16[16,128,128]{2,1,0:T(8,128)(2,1)} %bitcast_bitcast_fusion), calls=%async_computation.6 | async-start | bytes 1048576 | tf_op jit(solution)/shard_map/all_to_all | solution.py:214
  180.2 13.3 %all-to-all-done.5 = bf16[16,128,128]{2,1,0:T(8,128)(2,1)S(1)} async-done(((bf16[16,128,128]{2,1,0:T(8,128)(2,1)}), bf16[16,128,128]{2,1,0:T(8,128)(2,1)S(1)}, u32[]{:S(2)}, u32[]{:S(2)}) %all-to-all-start.5) | async-done | bytes 524320 | tf_op jit(solution)/shard_map/all_to_all | solution.py:214
  194.1 3.9 %all-to-all-start.9 = ((f32[16,1,16]{2,1,0:T(1,128)}), f32[16,1,16]{2,1,0:T(1,128)S(1)}, u32[]{:S(2)}, u32[]{:S(2)}) async-start(f32[16,1,16]{2,1,0:T(1,128)} %broadcast_in_dim.100), calls=%async_computation.10 | async-start | bytes 16384 | tf_op jit(solution)/shard_map/all_to_all | solution.py:51
  200.4 4.9 %all-to-all-done.9 = f32[16,1,16]{2,1,0:T(1,128)S(1)} async-done(((f32[16,1,16]{2,1,0:T(1,128)}), f32[16,1,16]{2,1,0:T(1,128)S(1)}, u32[]{:S(2)}, u32[]{:S(2)}) %all-to-all-start.9) | async-done | bytes 1056 | tf_op jit(solution)/shard_map/all_to_all | solution.py:51
  205.9 3.7 %all-to-all-start.3 = ((bf16[16,32,1024]{2,1,0:T(8,128)(2,1)}), bf16[16,32,1024]{2,1,0:T(8,128)(2,1)S(1)}, u32[]{:S(2)}, u32[]{:S(2)}) async-start(bf16[16,32,1024]{2,1,0:T(8,128)(2,1)} %bitcast.25), calls=%async_computation.4 | async-start | bytes 2097152 | tf_op jit(solution)/shard_map/all_to_all | solution.py:124
  209.6 4.6 %fusion.2 = bf16[1,512,2048]{2,1,0:T(8,128)(2,1)} fusion(bf16[512,2048]{0,1:T(8,128)(2,1)} %bitcast.221, bf16[1,512,512]{2,1,0:T(8,128)(2,1)S(1)} %copy-done.48, bf16[1,512,512]{2,1,0:T(8,128)(2,1)S(1)} %copy-done.51), kind=kOutput, calls=%fused_computation.7 | convolution fusion | flops 1077936128 | bytes 5242880 | tf_op jit(solution)/shard_map/rf,rd->fd/dot_general | solution.py:205
  218.2 3.7 %fusion.94 = f32[128,1024]{1,0:T(8,128)} fusion(bf16[2048,128]{1,0:T(8,128)(2,1)S(1)} %bitcast.217, bf16[2048,1024]{1,0:T(8,128)(2,1)} %all-gather.2.cloned.1.call-done), kind=kOutput, calls=%fused_computation.155 | convolution fusion | flops 536870912 | bytes 5242880 | tf_op jit(solution)/shard_map/td,ti->di/dot_general | solution.py:221
  222.8 9.2 %all-to-all-done.3 = bf16[16,32,1024]{2,1,0:T(8,128)(2,1)S(1)} async-done(((bf16[16,32,1024]{2,1,0:T(8,128)(2,1)}), bf16[16,32,1024]{2,1,0:T(8,128)(2,1)S(1)}, u32[]{:S(2)}, u32[]{:S(2)}) %all-to-all-start.3) | async-done | bytes 1048608 | tf_op jit(solution)/shard_map/all_to_all | solution.py:124
  232.2 6.3 %all_to_all.60 = bf16[2,512,1024]{2,1,0:T(8,128)(2,1)} all-to-all(bf16[2,512,1024]{2,1,0:T(8,128)(2,1)S(1)} %pad_maximum_fusion.1), channel_id=1, replica_groups=mesh['sp'=16,'tp'=2] {'tp'}, dimensions={0} | all-to-all | bytes 4194304 | tf_op jit(solution)/shard_map/all_to_all | solution.py:134
  238.6 2.9 %copy.142 = bf16[512,2,1024]{0,2,1:T(8,128)(2,1)S(1)} copy(bf16[512,2,1024]{2,0,1:T(8,128)(2,1)} %bitcast.203) | data formatting | bytes 4194304 | tf_op jit(solution)/shard_map/reshape | solution.py:133
  245.4 4.6 %fusion = bf16[1,2048,512]{2,1,0:T(8,128)(2,1)} fusion(bf16[512,2048]{0,1:T(8,128)(2,1)} %bitcast.223, bf16[1,512,512]{2,1,0:T(8,128)(2,1)S(1)} %copy-done.49, f32[512,512]{1,0:T(8,128)S(1)} %copy-done.54, bf16[1,512,512]{2,1,0:T(8,128)(2,1)S(1)} %copy-done.52), kind=kOutput, calls=%fused_computation.5 | convolution fusion | flops 1079508992 | bytes 6291456 | tf_op jit(solution)/shard_map/rd,rf->df/dot_general | solution.py:208
  (194 shorter events, 49.3 us)
Async XLA Ops:
  8.0 53.3 %copy-start = (bf16[1,2048,512]{2,1,0:T(8,128)(2,1)S(1)}, bf16[1,2048,512]{2,1,0:T(8,128)(2,1)}, u32[]{:S(2)}) copy-start(bf16[1,2048,512]{2,1,0:T(8,128)(2,1)} %param.23) | copy-start | bytes 6291460
  8.0 66.2 %reduce-scatter.2.cloned.1.call-start = ((), (), s32[]{:S(2)}) async-start(), calls=%async_computation.11 | async-start | bytes 3145728 | tf_op jit(solution)/shard_map/reduce_scatter | solution.py:152
  10.3 36.7 %copy-start.41 = (s32[2,128]{1,0:T(2,128)}, s32[2,128]{1,0:T(2,128)S(1)}, u32[]{:S(2)}) copy-start(s32[2,128]{1,0:T(2,128)S(1)} %add_bitcast_fusion) | copy-start | bytes 3076
  74.3 11.5 %copy-start.27 = (bf16[128,2048]{1,0:T(8,128)(2,1)S(1)}, bf16[128,2048]{1,0:T(8,128)(2,1)}, u32[]{:S(2)}) copy-start(bf16[128,2048]{1,0:T(8,128)(2,1)} %param.17) | copy-start | bytes 1572868
  74.3 37.3 %all-to-all-start.2 = ((bf16[16,32,1024]{2,1,0:T(8,128)(2,1)}), bf16[16,32,1024]{2,1,0:T(8,128)(2,1)}, u32[]{:S(2)}, u32[]{:S(2)}) async-start(bf16[16,32,1024]{2,1,0:T(8,128)(2,1)} %bitcast.228), calls=%async_computation.3 | async-start | bytes 2097152 | tf_op jit(solution)/shard_map/all_to_all | solution.py:155
  81.4 136.8 %all-gather.2.cloned.1.call-start = ((), (), s32[]{:S(2)}) async-start(), calls=%async_computation.12 | async-start | bytes 4456448 | tf_op jit(solution)/shard_map/all_gather | solution.py:193
  85.7 33.2 %copy-start.19 = (bf16[512,128]{1,0:T(8,128)(2,1)}, bf16[512,128]{1,0:T(8,128)(2,1)S(1)}, u32[]{:S(2)}) copy-start(bf16[512,128]{1,0:T(8,128)(2,1)S(1)} %fusion.62) | copy-start | bytes 393220
  112.9 19.0 %all-to-all-start.6 = ((f32[16,1,16]{2,1,0:T(1,128)}), f32[16,1,16]{2,1,0:T(1,128)}, u32[]{:S(2)}, u32[]{:S(2)}) async-start(f32[16,1,16]{2,1,0:T(1,128)} %broadcast_in_dim.61), calls=%async_computation.7 | async-start | bytes 16384 | tf_op jit(solution)/shard_map/all_to_all | solution.py:51
  130.6 8.2 %copy-start.42 = (pred[16,16]{1,0:T(8,128)(4,1)S(1)}, pred[16,16]{1,0:T(8,128)(4,1)}, u32[]{:S(2)}) copy-start(pred[16,16]{1,0:T(8,128)(4,1)} %get-tuple-element.82) | copy-start | bytes 772
  130.6 8.2 %copy-start.43 = (pred[16,16]{1,0:T(8,128)(4,1)S(1)}, pred[16,16]{1,0:T(8,128)(4,1)}, u32[]{:S(2)}) copy-start(pred[16,16]{1,0:T(8,128)(4,1)} %get-tuple-element.83) | copy-start | bytes 772
  131.9 21.6 %all-to-all-start.7 = ((bf16[16,64,128]{2,1,0:T(8,128)(2,1)}), bf16[16,64,128]{2,1,0:T(8,128)(2,1)S(1)}, u32[]{:S(2)}, u32[]{:S(2)}) async-start(bf16[16,64,128]{2,1,0:T(8,128)(2,1)} %bitcast.43), calls=%async_computation.8 | async-start | bytes 524288 | tf_op jit(solution)/shard_map/all_to_all | solution.py:75
  153.6 25.2 %copy-start.14 = (bf16[128,4,128]{2,1,0:T(4,128)(2,1)S(1)}, bf16[128,4,128]{2,1,0:T(4,128)(2,1)}, u32[]{:S(2)}) copy-start(bf16[128,4,128]{2,1,0:T(4,128)(2,1)} %copy-done.13) | copy-start | bytes 393220
  156.8 18.2 %all-to-all-start.8 = ((bf16[16,64,128]{2,1,0:T(8,128)(2,1)}), bf16[16,64,128]{2,1,0:T(8,128)(2,1)S(1)}, u32[]{:S(2)}, u32[]{:S(2)}) async-start(bf16[16,64,128]{2,1,0:T(8,128)(2,1)} %multiply_reduce_fusion), calls=%async_computation.9 | async-start | bytes 524288 | tf_op jit(solution)/shard_map/all_to_all | solution.py:83
  163.8 15.2 %copy-start.30 = (f32[128,16]{0,1:T(8,128)S(1)}, f32[128,16]{0,1:T(8,128)}, u32[]{:S(2)}) copy-start(f32[128,16]{0,1:T(8,128)} %get-tuple-element.77) | copy-start | bytes 24580
  175.1 18.4 %all-to-all-start.5 = ((bf16[16,128,128]{2,1,0:T(8,128)(2,1)}), bf16[16,128,128]{2,1,0:T(8,128)(2,1)S(1)}, u32[]{:S(2)}, u32[]{:S(2)}) async-start(bf16[16,128,128]{2,1,0:T(8,128)(2,1)} %bitcast_bitcast_fusion), calls=%async_computation.6 | async-start | bytes 1048576 | tf_op jit(solution)/shard_map/all_to_all | solution.py:214
  178.7 21.7 %copy-start.35 = (f32[128,16]{0,1:T(8,128)}, f32[128,16]{0,1:T(8,128)S(1)}, u32[]{:S(2)}) copy-start(f32[128,16]{0,1:T(8,128)S(1)} %multiply_reduce_fusion.2) | copy-start | bytes 24580
  178.8 19.3 %copy-start.20 = (bf16[512,128]{1,0:T(8,128)(2,1)S(1)}, bf16[512,128]{1,0:T(8,128)(2,1)}, u32[]{:S(2)}) copy-start(bf16[512,128]{1,0:T(8,128)(2,1)} %copy-done.19) | copy-start | bytes 393220
  180.1 25.2 %copy-start.37 = (f32[128,16]{0,1:T(8,128)}, f32[128,16]{0,1:T(8,128)S(1)}, u32[]{:S(2)}) copy-start(f32[128,16]{0,1:T(8,128)S(1)} %get-tuple-element.75) | copy-start | bytes 24580
  180.1 29.5 %copy-start.48 = (bf16[1,512,512]{2,1,0:T(8,128)(2,1)S(1)}, bf16[1,512,512]{2,1,0:T(8,128)(2,1)}, u32[]{:S(2)}) copy-start(bf16[1,512,512]{2,1,0:T(8,128)(2,1)} %param.21) | copy-start | bytes 1572868
  180.1 29.5 %copy-start.51 = (bf16[1,512,512]{2,1,0:T(8,128)(2,1)S(1)}, bf16[1,512,512]{2,1,0:T(8,128)(2,1)}, u32[]{:S(2)}) copy-start(bf16[1,512,512]{2,1,0:T(8,128)(2,1)} %param.22) | copy-start | bytes 1572868
  193.5 11.8 %copy-start.9 = (bf16[16,128,128]{2,1,0:T(8,128)(2,1)}, bf16[16,128,128]{2,1,0:T(8,128)(2,1)S(1)}, u32[]{:S(2)}) copy-start(bf16[16,128,128]{2,1,0:T(8,128)(2,1)S(1)} %all-to-all-done.5) | copy-start | bytes 1572868
  194.1 11.2 %all-to-all-start.9 = ((f32[16,1,16]{2,1,0:T(1,128)}), f32[16,1,16]{2,1,0:T(1,128)S(1)}, u32[]{:S(2)}, u32[]{:S(2)}) async-start(f32[16,1,16]{2,1,0:T(1,128)} %broadcast_in_dim.100), calls=%async_computation.10 | async-start | bytes 16384 | tf_op jit(solution)/shard_map/all_to_all | solution.py:51
  205.9 26.1 %all-to-all-start.3 = ((bf16[16,32,1024]{2,1,0:T(8,128)(2,1)}), bf16[16,32,1024]{2,1,0:T(8,128)(2,1)S(1)}, u32[]{:S(2)}, u32[]{:S(2)}) async-start(bf16[16,32,1024]{2,1,0:T(8,128)(2,1)} %bitcast.25), calls=%async_computation.4 | async-start | bytes 2097152 | tf_op jit(solution)/shard_map/all_to_all | solution.py:124
  209.6 4.9 %copy-start.33 = (pred[128,128]{1,0:T(8,128)(4,1)S(1)}, pred[128,128]{1,0:T(8,128)(4,1)}, u32[]{:S(2)}) copy-start(pred[128,128]{1,0:T(8,128)(4,1)} %copy-done.32) | copy-start | bytes 49156
  (40 other events, 94.3 us)
Sparse Core Ops, SparseCore 0:
  66.3 7.9 reduce-scatter.1
Sparse Core Ops, SparseCore 1:
  84.6 87.4 all-gather.1
